TPU v7x, 32 devices: a whole 2x2x4 slice. The times are simulated.
32 devices in a mesh: sp: 8 (over z, x), tp: 4 (over y, core).
Axes of the slice: x: 2, y: 2, z: 4, core: 2. Of those that a mesh axis runs over, the one named last changes fastest.
Arguments:
- tokens: bfloat16 [6144, 4096], P('sp', 'tp'), may hold values from -12 to 12
- query_weight: bfloat16 [4096, 2048], P(None, 'tp'), may hold values from -0.09375 to 0.09375
- key_weight: bfloat16 [4096, 2048], P(None, 'tp'), may hold values from -0.09375 to 0.09375
- value_weight: bfloat16 [4096, 2048], P(None, 'tp'), may hold values from -0.09375 to 0.09375
- position_bias: float32 [16, 320], P('tp'), may hold values from -104 to 154
- out_grad: bfloat16 [6144, 2048], P('sp', 'tp'), may hold values from -6 to 6
Outputs:
- input_grad: bfloat16 [6144, 4096], P('sp', 'tp')
- query_weight_grad: float32 [4096, 2048], P('sp', 'tp')
- key_weight_grad: float32 [4096, 2048], P('sp', 'tp')
- value_weight_grad: float32 [4096, 2048], P('sp', 'tp')
- bias_grad: float32 [16, 320], P('tp')
All inputs are finite; a program needn't handle non-finite values.
Results may differ from a plain program's by a relative error of at most 0.014.
Values may be sent and summed in bfloat16 or wider, within the bound.
No kernel may reach another device: no remote copies, remote signals or barrier semaphores. Data moves between devices by JAX's collectives and lax.ppermute only.
A program may use at most 128 MiB of HBM per device.

v0:
```python
import jax
import jax.numpy as jnp
import numpy as np
from jax import lax
from jax.sharding import PartitionSpec as P

SEGMENT = 64
PREVIOUS = 4
CLIP = 256


def from_behind(value, axis, steps):
    count = lax.axis_size(axis)
    leading, last = (max(0, -steps), min(count, count - steps))
    return lax.ppermute(value, axis, [(source, source + steps) for source in range(leading, last)])


def band_view(extended, count, heads, head):
    shaped = extended.reshape(count + PREVIOUS, SEGMENT, heads, head)
    stacked = jnp.stack([shaped[band : band + count] for band in range(PREVIOUS + 1)], axis=1)
    return stacked.reshape(count, (PREVIOUS + 1) * SEGMENT, heads, head)


def fold_band(parts, count):
    heads = parts.shape[2]
    head = parts.shape[3]
    shaped = parts.reshape(count, PREVIOUS + 1, SEGMENT, heads, head)
    total = jnp.zeros((count + PREVIOUS, SEGMENT, heads, head), jnp.float32)
    for band in range(PREVIOUS + 1):
        total = total + jnp.pad(shaped[:, band], ((band, PREVIOUS - band), (0, 0), (0, 0), (0, 0)))
    return total.reshape((count + PREVIOUS) * SEGMENT, heads * head)


def diagonal_table(reach, table_len):
    diagonals = reach + 2 * SEGMENT - 1
    distance = reach + SEGMENT - 1 - np.arange(diagonals)
    target = np.minimum(distance, CLIP) + SEGMENT - 1
    return (
        target.astype(np.int32),
        (target[:, None] == np.arange(table_len)[None, :]).astype(np.float32),
    )


def contract_rows(left, right):
    return lax.dot_general(
        left, right, (((0,), (0,)), ((), ())), preferred_element_type=jnp.float32
    )


def contract_cols(left, right):
    return lax.dot_general(
        left, right, (((1,), (1,)), ((), ())), preferred_element_type=jnp.float32
    )


def shards(tokens, query_weight, key_weight, value_weight, position_bias, out_grad):
    whole = lax.all_gather(tokens, "tp", axis=1, tiled=True)
    query = jnp.dot(whole, query_weight, preferred_element_type=jnp.float32).astype(jnp.bfloat16)
    keys = jnp.dot(whole, key_weight, preferred_element_type=jnp.float32).astype(jnp.bfloat16)
    values = jnp.dot(whole, value_weight, preferred_element_type=jnp.float32).astype(jnp.bfloat16)
    length, width = query.shape
    heads = position_bias.shape[0]
    head = width // heads
    reach = PREVIOUS * SEGMENT
    span = reach + SEGMENT
    count = length // SEGMENT
    factor = head ** (-0.5)
    prev_keys, prev_values = from_behind(
        (keys[length - reach :], values[length - reach :]), "sp", 1
    )
    key_band = band_view(jnp.concatenate([prev_keys, keys]), count, heads, head)
    value_band = band_view(jnp.concatenate([prev_values, values]), count, heads, head)
    query_seg = query.reshape(count, SEGMENT, heads, head)
    grad_seg = out_grad.reshape(count, SEGMENT, heads, head)
    target, fold_map = diagonal_table(reach, position_bias.shape[1])
    along = position_bias[:, target]
    bias = jnp.stack(
        [along[:, SEGMENT - 1 - row : SEGMENT - 1 - row + span] for row in range(SEGMENT)], axis=1
    )
    scores = (
        jnp.einsum("cqhd,ckhd->hcqk", query_seg, key_band, preferred_element_type=jnp.float32)
        * factor
        + bias[:, None]
    )
    offset = lax.axis_index("sp") * length
    key_pos = offset - reach + jnp.arange(count)[:, None] * SEGMENT + jnp.arange(span)[None, :]
    valid = (key_pos >= 0)[None, :, None, :]
    masked = jnp.where(valid, scores, -jnp.inf)
    top = jnp.max(masked, axis=-1, keepdims=True)
    logsum = top + jnp.log(jnp.sum(jnp.exp(masked - top), axis=-1, keepdims=True))
    weights = jnp.exp(masked - logsum)
    weights_low = weights.astype(jnp.bfloat16)
    prob_grad = jnp.einsum(
        "cqhd,ckhd->hcqk", grad_seg, value_band, preferred_element_type=jnp.float32
    )
    delta = jnp.sum(weights * prob_grad, axis=-1, keepdims=True)
    score_grad = weights * (prob_grad - delta)
    score_low = score_grad.astype(jnp.bfloat16)
    query_grad = (
        (
            jnp.einsum("hcqk,ckhd->cqhd", score_low, key_band, preferred_element_type=jnp.float32)
            * factor
        )
        .reshape(length, width)
        .astype(jnp.bfloat16)
    )
    key_parts = (
        jnp.einsum("hcqk,cqhd->ckhd", score_low, query_seg, preferred_element_type=jnp.float32)
        * factor
    )
    value_parts = jnp.einsum(
        "hcqk,cqhd->ckhd", weights_low, grad_seg, preferred_element_type=jnp.float32
    )
    key_total = fold_band(key_parts, count)
    value_total = fold_band(value_parts, count)
    back_keys, back_values = from_behind((key_total[:reach], value_total[:reach]), "sp", -1)
    edge_pad = ((length - reach, 0), (0, 0))
    key_grad = (key_total[reach:] + jnp.pad(back_keys, edge_pad)).astype(jnp.bfloat16)
    value_grad = (value_total[reach:] + jnp.pad(back_values, edge_pad)).astype(jnp.bfloat16)
    bias_terms = jnp.sum(score_grad, axis=1)[:, ::-1, :]
    skewed = jnp.pad(bias_terms, ((0, 0), (0, 0), (0, SEGMENT))).reshape(
        heads, SEGMENT * (span + SEGMENT)
    )
    skewed = skewed[:, : SEGMENT * (span + SEGMENT - 1)].reshape(heads, SEGMENT, span + SEGMENT - 1)
    diagonal_sums = jnp.sum(skewed, axis=1)
    bias_local = jnp.dot(
        diagonal_sums,
        jnp.asarray(fold_map),
        precision=lax.Precision.HIGHEST,
        preferred_element_type=jnp.float32,
    )
    bias_grad = lax.psum(bias_local, "sp")
    input_part = (
        contract_cols(query_grad, query_weight)
        + contract_cols(key_grad, key_weight)
        + contract_cols(value_grad, value_weight)
    )
    input_grad = lax.psum_scatter(
        input_part.astype(jnp.bfloat16), "tp", scatter_dimension=1, tiled=True
    )
    stacked = jnp.concatenate([query_grad, key_grad, value_grad], axis=1)
    weight_grad = lax.psum_scatter(
        contract_rows(whole, stacked), "sp", scatter_dimension=0, tiled=True
    )
    return (
        input_grad,
        weight_grad[:, :width],
        weight_grad[:, width : 2 * width],
        weight_grad[:, 2 * width :],
        bias_grad,
    )


def solution(mesh):
    in_specs = (
        P("sp", "tp"),
        P(None, "tp"),
        P(None, "tp"),
        P(None, "tp"),
        P("tp", None),
        P("sp", "tp"),
    )
    out_specs = (P("sp", "tp"), P("sp", "tp"), P("sp", "tp"), P("sp", "tp"), P("tp", None))
    return jax.shard_map(shards, mesh=mesh, in_specs=in_specs, out_specs=out_specs, check_vma=False)
```

profile of v0, /device:TPU:0, one launch (start us, length us, event | category | flops | bytes accessed | tf_op | source)
XLA Modules:
  0.0 686.2 jit_solution(1822297870764970203)
XLA Ops:
  9.5 1.1 gather_fusion
  42.7 15.9 %all-gather.2.cloned.1.call-done = bf16[768,4096]{1,0:T(8,128)(2,1)} async-done(((bf16[768,1024]{1,0:T(8,128)(2,1)}), bf16[768,4096]{1,0:T(8,128)(2,1)}) %all-gather.2.cloned.1.call-update) | async-done | bytes 6291472 | tf_op jit(solution)/shard_map/all_gather | solution.py:57
  58.7 7.5 %convolution_convert_fusion.2 = bf16[768,512]{1,0:T(8,128)(2,1)S(1)} fusion(bf16[768,4096]{1,0:T(8,128)(2,1)} %all-gather.2.cloned.1.call-done, bf16[4096,512]{1,0:T(8,128)(2,1)} %param.11), kind=kOutput, calls=%fused_computation.48 | convolution fusion | flops 3221618688 | bytes 11272192 | tf_op jit(solution)/shard_map/dot_general | solution.py:59
  66.9 4.5 collective-permute-start
  71.4 3.4 convolution_convert_fusion.1
  74.9 3.4 convolution_convert_fusion
  78.3 1.1 stack.235
  80.1 1.1 stack.306
  81.4 3.4 collective-permute-start.1
  84.8 2.6 pad_maximum_fusion.1
  87.4 2.5 stack.231
  89.9 2.4 constant_dynamic-update-slice_fusion.4
  92.3 2.4 stack.232
  94.7 1.1 stack.233
  95.8 1.1 stack.234
  96.8 2.5 constant_dynamic-update-slice_fusion.3
  99.3 1.2 constant_dynamic-update-slice_fusion.2
  100.6 1.2 constant_dynamic-update-slice_fusion.1
  101.8 1.2 constant_dynamic-update-slice_fusion
  103.0 3.2 copy.152
  106.2 1.6 fusion.38
  107.8 1.3 exponential_reduce_fusion
  109.9 2.5 fusion.8
  112.5 1.5 fusion.34
  114.0 1.0 copy.294
  115.0 2.5 copy_bitcast_fusion.2
  117.5 2.5 copy_bitcast_fusion
  120.2 1.9 copy-done.1
  122.1 3.0 copy.241
  125.9 1.3 collective-permute-start.3
  127.2 1.5 pad_add_fusion
  129.8 2.8 pad_maximum_fusion
  132.7 2.5 stack.302
  135.1 2.4 constant_dynamic-update-slice_fusion.9
  137.5 2.4 stack.303
  139.9 2.4 stack.304
  142.4 2.4 stack.305
  144.8 2.5 constant_dynamic-update-slice_fusion.8
  147.3 2.4 constant_dynamic-update-slice_fusion.7
  149.6 1.2 constant_dynamic-update-slice_fusion.6
  150.8 1.2 constant_dynamic-update-slice_fusion.5
  152.0 3.3 copy.219
  155.4 1.5 fusion.29
  156.9 17.5 %fusion.36 = (f32[4,64,320]{2,1,0:T(8,128)S(1)}, bf16[4,12,64,320]{3,2,1,0:T(8,128)(2,1)S(1)}) fusion(f32[4,12,320,64]{2,3,1,0:T(8,128)S(1)} %fusion.29, f32[4,12,64,320]{3,2,1,0:T(8,128)S(1)} %bitcast.228, f32[4,12,64]{2,1,0:T(8,128)S(1)} %copy-done.16), kind=kOutput, calls=%fused_computation.157 | output fusion | flops 6802751 | bytes 10170368 | tf_op jit(solution)/shard_map/sub | solution.py:97
  174.4 1.3 broadcast_multiply_fusion
  175.7 1.5 fusion.35
  178.3 2.5 copy_bitcast_fusion.7
  180.8 2.5 copy_bitcast_fusion.5
  183.3 1.1 pad_add_fusion.1
  184.7 1.6 collective-permute-start.2
  186.2 1.1 copy-done.2
  189.1 1.3 fusion.13
  190.4 10.7 %collective-permute-done.2 = f32[256,512]{1,0:T(8,128)S(1)} collective-permute-done((f32[256,512]{1,0:T(8,128)S(1)}, f32[256,512]{1,0:T(8,128)S(1)}, u32[]{:S(2)}, u32[]{:S(2)}) %collective-permute-start.2) | collective-permute-done | bytes 524320 | tf_op jit(solution)/shard_map/ppermute | solution.py:15
  201.3 13.9 %convolution_bitcast_fusion = f32[4096,1536]{0,1:T(8,128)} fusion(bf16[768,4096]{1,0:T(8,128)(2,1)S(1)} %bitcast.248, bf16[768,512]{1,0:T(8,128)(2,1)S(1)} %fusion.13, bf16[768,512]{1,0:T(8,128)(2,1)S(1)} %fusion.14, bf16[768,512]{1,0:T(8,128)(2,1)S(1)} %bitcast.245), kind=kOutput, calls=%fused_computation.2 | convolution fusion | flops 9670754304 | bytes 33816576 | tf_op jit(solution)/shard_map/dot_general | solution.py:45
  215.3 9.3 %fusion.33 = f32[768,4096]{1,0:T(8,128)} fusion(bf16[4096,512]{1,0:T(8,128)(2,1)} %param.10, bf16[96,8,4,128]{3,2,1,0:T(4,128)(2,1)S(1)} %bitcast.241), kind=kOutput, calls=%fused_computation.154 | convolution fusion | flops 3221225472 | bytes 17563648 | tf_op jit(solution)/shard_map/dot_general | solution.py:51
  224.6 6.4 fusion.39
  231.0 14.1 %add_convert_fusion = bf16[768,4096]{1,0:T(8,128)(2,1)} fusion(f32[768,4096]{1,0:T(8,128)} %fusion.33, f32[768,4096]{1,0:T(8,128)} %fusion.39, bf16[768,512]{1,0:T(8,128)(2,1)S(1)} %fusion.13, bf16[4096,512]{1,0:T(8,128)(2,1)} %param.12), kind=kOutput, calls=%fused_computation.3 | convolution fusion | flops 3230662656 | bytes 36438016 | tf_op jit(solution)/shard_map/dot_general | solution.py:51
  246.6 22.0 %psum.7 = f32[4,320]{1,0:T(4,128)} all-reduce(f32[4,320]{1,0:T(4,128)S(1)} %fusion.40), channel_id=1, replica_groups=mesh['sp'=8,'tp'=4] {'sp'}, use_global_device_ids=true, to_apply=%region_7.8 | all-reduce | flops 1280 | bytes 10240 | tf_op jit(solution)/shard_map/psum | solution.py:132
  268.6 350.7 %reduce-scatter.5.cloned.1.call-done = f32[512,1536]{0,1:T(8,128)} async-done(((f32[4096,1536]{0,1:T(8,128)}), f32[512,1536]{0,1:T(8,128)}) %reduce-scatter.5.cloned.1.call-update) | async-done | bytes 3145744 | tf_op jit(solution)/shard_map/reduce_scatter | solution.py:142
  619.3 2.2 fusion.37
  621.5 1.3 copy.238
  622.8 1.3 copy.239
  624.1 1.3 copy.240
  625.4 54.1 %reduce-scatter.3.cloned.1.call-done = bf16[768,1024]{1,0:T(8,128)(2,1)} async-done(((bf16[768,4096]{1,0:T(8,128)(2,1)}), bf16[768,1024]{1,0:T(8,128)(2,1)}) %reduce-scatter.3.cloned.1.call-update) | async-done | bytes 1572880 | tf_op jit(solution)/shard_map/reduce_scatter | solution.py:138
  (229 shorter events, 43.0 us)
Async XLA Ops:
  7.2 51.5 %all-gather.2.cloned.1.call-start = ((), (), s32[]{:S(2)}) async-start(), calls=%async_computation.2 | async-start | bytes 7864320 | tf_op jit(solution)/shard_map/all_gather | solution.py:57
  7.9 611.4 %reduce-scatter.5.cloned.1.call-start = ((), (), s32[]{:S(2)}) async-start(), calls=%async_computation.4 | async-start | bytes 28311552 | tf_op jit(solution)/shard_map/reduce_scatter | solution.py:142
  39.3 2.1 copy-start.13
  40.1 1.5 copy-start.17
  40.1 1.5 copy-start.18
  40.1 1.5 copy-start.19
  40.1 1.5 copy-start.20
  40.1 1.5 copy-start.21
  40.1 1.5 copy-start.22
  40.1 1.5 copy-start.23
  40.2 1.5 copy-start.24
  40.2 1.5 copy-start.25
  40.2 1.5 copy-start.26
  40.2 1.5 copy-start.27
  40.2 1.5 copy-start.28
  40.2 1.5 copy-start.29
  40.2 1.5 copy-start.30
  40.2 1.5 copy-start.31
  40.2 1.5 copy-start.32
  40.2 1.5 copy-start.33
  40.3 1.5 copy-start.34
  40.3 1.5 copy-start.35
  40.3 1.5 copy-start.36
  40.3 1.5 copy-start.37
  40.3 1.5 copy-start.38
  40.3 1.5 copy-start.39
  40.3 1.5 copy-start.40
  40.3 1.5 copy-start.41
  40.3 1.5 copy-start.42
  40.3 1.5 copy-start.43
  40.4 1.5 copy-start.44
  40.4 1.5 copy-start.45
  40.4 1.5 copy-start.46
  40.4 1.5 copy-start.47
  40.4 1.5 copy-start.48
  40.4 1.5 copy-start.49
  40.4 1.5 copy-start.50
  58.7 12.8 %copy-start.55 = (bf16[768,4096]{1,0:T(8,128)(2,1)S(1)}, bf16[768,4096]{1,0:T(8,128)(2,1)}, u32[]{:S(2)}) copy-start(bf16[768,4096]{1,0:T(8,128)(2,1)} %all-gather.2.cloned.1.call-done) | copy-start | bytes 18874372
  58.7 12.8 %copy-start.56 = (bf16[4096,512]{1,0:T(8,128)(2,1)S(1)}, bf16[4096,512]{1,0:T(8,128)(2,1)}, u32[]{:S(2)}) copy-start(bf16[4096,512]{1,0:T(8,128)(2,1)} %param.10) | copy-start | bytes 12582916
  66.9 7.9 %copy-start.6 = (bf16[4096,512]{1,0:T(8,128)(2,1)S(1)}, bf16[4096,512]{1,0:T(8,128)(2,1)}, u32[]{:S(2)}) copy-start(bf16[4096,512]{1,0:T(8,128)(2,1)} %param.12) | copy-start | bytes 12582916
  66.9 17.9 %collective-permute-start = (bf16[256,512]{1,0:T(8,128)(2,1)}, bf16[256,512]{1,0:T(8,128)(2,1)}, u32[]{:S(2)}, u32[]{:S(2)}) collective-permute-start(bf16[256,512]{1,0:T(8,128)(2,1)} %slice.398), channel_id=1, source_target_pairs={{0,4},{4,8},{8,12},{12,16},{16,20},{20,24},{24,28},{1,5},{5,9},{9,... | collective-permute-start | bytes 786440 | tf_op jit(solution)/shard_map/ppermute | solution.py:15
  78.3 1.9 copy-start.4
  81.4 47.4 %collective-permute-start.1 = (bf16[256,512]{1,0:T(8,128)(2,1)}, bf16[256,512]{1,0:T(8,128)(2,1)}, u32[]{:S(2)}, u32[]{:S(2)}) collective-permute-start(bf16[256,512]{1,0:T(8,128)(2,1)} %slice.469), channel_id=1, source_target_pairs={{0,4},{4,8},{8,12},{12,16},{16,20},{20,24},{24,28},{1,5},{5,9},{9,... | collective-permute-start | bytes 786440 | tf_op jit(solution)/shard_map/ppermute | solution.py:15
  87.4 7.3 %copy-start.7 = (bf16[768,512]{1,0:T(8,128)(2,1)S(1)}, bf16[768,512]{1,0:T(8,128)(2,1)}, u32[]{:S(2)}) copy-start(bf16[768,512]{1,0:T(8,128)(2,1)} %get-tuple-element.47) | copy-start | bytes 2359300
  95.8 3.6 copy-start.10
  96.8 3.7 copy-start.11
  96.8 5.0 copy-start.9
  107.8 2.2 copy-start
  109.9 2.5 copy-start.15
  120.0 2.1 copy-start.1
  125.9 63.2 %collective-permute-start.3 = (f32[256,512]{1,0:T(8,128)}, f32[256,512]{1,0:T(8,128)}, u32[]{:S(2)}, u32[]{:S(2)}) collective-permute-start(f32[256,512]{1,0:T(8,128)} %bitcast.220), channel_id=1, source_target_pairs={{4,0},{8,4},{12,8},{16,12},{20,16},{24,20},{28,24},{5,1},{9,5},{13... | collective-permute-start | bytes 1572872 | tf_op jit(solution)/shard_map/ppermute | solution.py:15
  144.8 4.8 copy-start.12
  144.8 6.0 copy-start.8
  152.0 4.8 slice-start
  155.3 1.5 slice-start.1
  155.4 1.5 copy-start.16
  184.4 1.8 copy-start.3
  184.6 2.7 copy-start.2
  184.6 16.7 %slice-start.3 = ((s8[6291456]{0:T(1024)(128)(4,1)}), s8[4194304]{0:T(1024)(128)(4,1)S(1)}, s32[]{:S(2)}) async-start(s8[6291456]{0:T(1024)(128)(4,1)} %bitcast.247), calls=%async_computation.8 | async-start | bytes 8388608
  184.7 16.4 %collective-permute-start.2 = (f32[256,512]{1,0:T(8,128)S(1)}, f32[256,512]{1,0:T(8,128)S(1)}, u32[]{:S(2)}, u32[]{:S(2)}) collective-permute-start(f32[256,512]{1,0:T(8,128)S(1)} %bitcast.246), channel_id=1, source_target_pairs={{4,0},{8,4},{12,8},{16,12},{20,16},{24,20},{28,24},{5,1},{9,5},{13... | collective-permute-start | bytes 1572872 | tf_op jit(solution)/shard_map/ppermute | solution.py:15
  187.3 14.0 %slice-start.4 = ((s8[6291456]{0:T(1024)(128)(4,1)}), s8[2097152]{0:T(1024)(128)(4,1)S(1)}, s32[]{:S(2)}) async-start(s8[6291456]{0:T(1024)(128)(4,1)} %bitcast.247), calls=%async_computation.9 | async-start | bytes 4194304
  188.9 12.2 %slice-start.2 = ((f32[16,64,4,128]{3,2,1,0:T(4,128)}), f32[12,64,4,128]{3,2,1,0:T(4,128)S(1)}, s32[]{:S(2)}) async-start(f32[16,64,4,128]{3,2,1,0:T(4,128)} %copy-done.3), calls=%async_computation.7 | async-start | bytes 3145728 | tf_op jit(solution)/shard_map/slice | solution.py:118
  215.3 464.2 %reduce-scatter.3.cloned.1.call-start = ((), (), s32[]{:S(2)}) async-start(), calls=%async_computation.3 | async-start | bytes 7864320 | tf_op jit(solution)/shard_map/reduce_scatter | solution.py:138
  215.3 9.3 %copy-start.57 = (bf16[4096,512]{1,0:T(8,128)(2,1)S(1)}, bf16[4096,512]{1,0:T(8,128)(2,1)}, u32[]{:S(2)}) copy-start(bf16[4096,512]{1,0:T(8,128)(2,1)} %param.11) | copy-start | bytes 12582916
  (6 other events, 8.1 us)
Sparse Core Ops, SparseCore 0:
  9.5 49.0 all-gather.1
  215.4 403.9 reduce-scatter.4
  622.5 56.9 reduce-scatter.2
where the time goes:
time: 693 us; the launch traced here: 686 us
  waiting for transfers between devices  432 us (62%)
  local copies, waits for them, and re-layouts  110 us (16%)
  matrix products  66.3 us (10%)
  other arithmetic  29.4 us (4%)
  blocking collectives  22 us (3%)
  between operations  15.2 us (2%)
  starting transfers between devices  10.9 us (2%)
    reduce_scatter x1, waiting for transfers between devices, shards(): lax.psum_scatter(contract_rows(whole, stacked), 'sp', scatter_dimension=0...  351 us
    reduce_scatter x1, waiting for transfers between devices, shards(): lax.psum_scatter(input_part.astype(jnp.bfloat16), 'tp', scatter_dimension...  54.1 us
    another operation x69, local copies, waits for them, and re-layouts, shards(): jnp.stack([along[:, SEGMENT - 1 - row:SEGMENT - 1 - row + span] for row i...  31 us
    dot_general x3, matrix products, contract_cols(): lax.dot_general(left, right, (((1,), (1,)), ((), ())), preferred_element_...  29.8 us
    unnamed x143, local copies, waits for them, and re-layouts  29 us
    another operation x14, local copies, waits for them, and re-layouts, band_view(): jnp.stack([shaped[band:band + count] for band in range(PREVIOUS + 1)], ax...  27.9 us
    psum x1, blocking collectives, shards(): bias_grad = lax.psum(bias_local, 'sp')  22 us
    sub x1, other arithmetic, shards(): score_grad = weights * (prob_grad - delta)  17.5 us
  transfers between devices with their start and end apart: 7, of which 4 were waited for; matrix products, arithmetic and copies ran while one was open for 26% of the time, Pallas kernels for 0%

commit v1 on v0

v1 whole, which is shorter than its diff:
```python
import jax
import jax.numpy as jnp
from jax import lax
from jax.experimental import pallas as pl
from jax.experimental.pallas import tpu as pltpu
from jax.sharding import PartitionSpec as P

SEGMENT = 64
PREVIOUS = 4
REACH = PREVIOUS * SEGMENT
SPAN = REACH + SEGMENT
ROWS = 2 * SEGMENT
KEYS = REACH + ROWS
LANES = KEYS


def from_behind(value, axis, steps):
    count = lax.axis_size(axis)
    leading, last = (max(0, -steps), min(count, count - steps))
    return lax.ppermute(value, axis, [(source, source + steps) for source in range(leading, last)])


def contract_rows(left, right):
    return lax.dot_general(
        left, right, (((0,), (0,)), ((), ())), preferred_element_type=jnp.float32
    )


def contract_cols(left, right):
    return lax.dot_general(
        left, right, (((1,), (1,)), ((), ())), preferred_element_type=jnp.float32
    )


def attention_kernel(
    first_ref, q_ref, k_ref, v_ref, pk_ref, pv_ref, g_ref, along_ref,
    dq_ref, dk_ref, dv_ref, hk_ref, hv_ref, diag_ref,
    kx, vx, dkx, dvx, acc, bias_t,
):
    length, head = q_ref.shape
    factor = head ** (-0.5)
    kx[:REACH] = pk_ref[...]
    kx[REACH:] = k_ref[...]
    vx[:REACH] = pv_ref[...]
    vx[REACH:] = v_ref[...]
    row = lax.broadcasted_iota(jnp.int32, (SEGMENT, LANES), 0)
    col = lax.broadcasted_iota(jnp.int32, (SEGMENT, LANES), 1)
    back = SEGMENT - 1 - row
    table = jnp.broadcast_to(along_ref[0], (SEGMENT, LANES))
    step = 1
    while step < SEGMENT:
        table = jnp.where((back & step) != 0, pltpu.roll(table, LANES - step, 1), table)
        step *= 2
    table = jnp.where(col < SPAN, table, -jnp.inf)
    bias_t[...] = jnp.concatenate([table, pltpu.roll(table, SEGMENT, 1)], axis=0).T
    acc[...] = jnp.zeros_like(acc)
    dkx[...] = jnp.zeros_like(dkx)
    dvx[...] = jnp.zeros_like(dvx)
    blind = first_ref[0] * REACH
    for start in range(0, length, ROWS):
        rows = pl.ds(start, ROWS)
        seen = pl.ds(start, KEYS)
        q = q_ref[rows, :]
        g = g_ref[rows, :]
        k = kx[seen, :]
        scores = contract_cols(k, q) * factor + bias_t[...]
        if start < REACH:
            place = lax.broadcasted_iota(jnp.int32, (KEYS, ROWS), 0) + start
            scores = jnp.where(place < blind, -jnp.inf, scores)
        prob_grad = contract_cols(vx[seen, :], g)
        top = jnp.max(scores, axis=0, keepdims=True)
        power = jnp.exp(scores - top)
        weights = power * (1.0 / jnp.sum(power, axis=0, keepdims=True))
        delta = jnp.sum(weights * prob_grad, axis=0, keepdims=True)
        score_grad = weights * (prob_grad - delta)
        acc[...] += score_grad
        weights_low = weights.astype(jnp.bfloat16)
        score_low = score_grad.astype(jnp.bfloat16)
        dvx[seen, :] += jnp.dot(weights_low, g, preferred_element_type=jnp.float32)
        dkx[seen, :] += jnp.dot(score_low, q, preferred_element_type=jnp.float32)
        dq_ref[rows, :] = (contract_rows(score_low, k) * factor).astype(jnp.bfloat16)
    hk_ref[...] = (dkx[:REACH] * factor).astype(jnp.bfloat16)
    hv_ref[...] = dvx[:REACH].astype(jnp.bfloat16)
    dk_ref[...] = dkx[REACH:] * factor
    dv_ref[...] = dvx[REACH:]
    both = acc[...].T
    skew = both[:SEGMENT] + pltpu.roll(both[SEGMENT:], LANES - SEGMENT, 1)
    step = 1
    while step < SEGMENT:
        skew = jnp.where((back & step) != 0, pltpu.roll(skew, step, 1), skew)
        step *= 2
    diag_ref[0] = jnp.sum(skew, axis=0, keepdims=True)


def attention(first, query, keys, values, prev_keys, prev_values, out_grad, table):
    length, width = query.shape
    heads = table.shape[0]
    head = width // heads
    along = jnp.concatenate(
        [
            jnp.broadcast_to(table[:, -1:], (heads, SEGMENT - 1)),
            table[:, ::-1],
            jnp.zeros((heads, LANES - SEGMENT + 1 - table.shape[1]), jnp.float32),
        ],
        axis=1,
    )[:, None, :]
    whole = pl.BlockSpec((length, head), lambda h: (0, h))
    edge = pl.BlockSpec((REACH, head), lambda h: (0, h))
    line = pl.BlockSpec((1, 1, LANES), lambda h: (h, 0, 0))
    flops = 2 * 5 * heads * length * KEYS * head
    outs = pl.pallas_call(
        attention_kernel,
        grid=(heads,),
        in_specs=[
            pl.BlockSpec(memory_space=pltpu.SMEM),
            whole, whole, whole, edge, edge, whole, line,
        ],
        out_specs=[whole, whole, whole, edge, edge, line],
        out_shape=[
            jax.ShapeDtypeStruct((length, width), jnp.bfloat16),
            jax.ShapeDtypeStruct((length, width), jnp.float32),
            jax.ShapeDtypeStruct((length, width), jnp.float32),
            jax.ShapeDtypeStruct((REACH, width), jnp.bfloat16),
            jax.ShapeDtypeStruct((REACH, width), jnp.bfloat16),
            jax.ShapeDtypeStruct((heads, 1, LANES), jnp.float32),
        ],
        scratch_shapes=[
            pltpu.VMEM((REACH + length, head), jnp.bfloat16),
            pltpu.VMEM((REACH + length, head), jnp.bfloat16),
            pltpu.VMEM((REACH + length, head), jnp.float32),
            pltpu.VMEM((REACH + length, head), jnp.float32),
            pltpu.VMEM((KEYS, ROWS), jnp.float32),
            pltpu.VMEM((KEYS, ROWS), jnp.float32),
        ],
        cost_estimate=pl.CostEstimate(
            flops=flops, bytes_accessed=12 * length * width, transcendentals=heads * length * KEYS
        ),
        compiler_params=pltpu.CompilerParams(vmem_limit_bytes=32 * 1024 * 1024),
        name="segment_attention",
    )(first, query, keys, values, prev_keys, prev_values, out_grad, along)
    diag = outs[-1][:, 0]
    size = table.shape[1]
    bias_grad = jnp.concatenate(
        [
            diag[:, SEGMENT : SEGMENT + size - 1][:, ::-1],
            jnp.sum(diag[:, :SEGMENT], axis=1, keepdims=True),
        ],
        axis=1,
    )
    return [*outs[:-1], bias_grad]


def shards(tokens, query_weight, key_weight, value_weight, position_bias, out_grad):
    whole = lax.all_gather(tokens, "tp", axis=1, tiled=True)
    length = whole.shape[0]
    cut = length - REACH

    def project(rows, weight):
        return jnp.dot(rows, weight, preferred_element_type=jnp.float32).astype(jnp.bfloat16)

    keys = project(whole, key_weight)
    values = project(whole, value_weight)
    prev_keys, prev_values = from_behind((keys[cut:], values[cut:]), "sp", 1)
    query = project(whole, query_weight)
    first = (lax.axis_index("sp") == 0).astype(jnp.int32).reshape(1)
    query_grad, key_own, value_own, key_back, value_back, bias_local = attention(
        first, query, keys, values, prev_keys, prev_values, out_grad, position_bias
    )
    back_keys, back_values = from_behind((key_back, value_back), "sp", -1)

    def join(own, back):
        return jnp.concatenate([own[:cut], own[cut:] + back.astype(jnp.float32)]).astype(
            jnp.bfloat16
        )

    def reduce_weight(grad):
        part = contract_rows(whole, grad).astype(jnp.bfloat16)
        return lax.psum_scatter(part, "sp", scatter_dimension=0, tiled=True).astype(jnp.float32)

    query_weight_grad = reduce_weight(query_grad)
    key_grad = join(key_own, back_keys)
    value_grad = join(value_own, back_values)
    key_weight_grad = reduce_weight(key_grad)
    value_weight_grad = reduce_weight(value_grad)
    input_part = (
        contract_cols(query_grad, query_weight)
        + contract_cols(key_grad, key_weight)
        + contract_cols(value_grad, value_weight)
    )
    input_grad = lax.psum_scatter(
        input_part.astype(jnp.bfloat16), "tp", scatter_dimension=1, tiled=True
    )
    bias_grad = lax.psum(bias_local, "sp")
    return input_grad, query_weight_grad, key_weight_grad, value_weight_grad, bias_grad


def solution(mesh):
    in_specs = (
        P("sp", "tp"),
        P(None, "tp"),
        P(None, "tp"),
        P(None, "tp"),
        P("tp", None),
        P("sp", "tp"),
    )
    out_specs = (P("sp", "tp"), P("sp", "tp"), P("sp", "tp"), P("sp", "tp"), P("tp", None))
    return jax.shard_map(shards, mesh=mesh, in_specs=in_specs, out_specs=out_specs, check_vma=False)
```

time: 693 us -> 451 us (0.65)
  waiting for transfers between devices: 432 us -> 301 us
  local copies, waits for them, and re-layouts: 110 us -> 13.4 us
  other arithmetic: 29.4 us -> 1.46 us
  Pallas kernels: 0 us -> 15.7 us
  blocking collectives: 22 us -> 29.6 us
    reduce_scatter x1 -> x3, waiting for transfers between devices: 351 us -> 170 us  [reduce_weight(): lax.psum_scatter(part, 'sp', scatter_dimension=0, tiled=True)]
    another operation x83 -> x0, local copies, waits for them, and re-layouts: 58.9 us -> none  [the longest x69 31 us: shards(): jnp.stack([along[:, SEGMENT - 1 - row:SEGMENT - 1 - row + span] for row i...]
    all_gather x1, waiting for transfers between devices: 15.9 us -> 48 us  [shards(): whole = lax.all_gather(tokens, 'tp', axis=1, tiled=True)]
    unnamed x143 -> x24, local copies, waits for them, and re-layouts: 29 us -> 10.8 us
    sub x1 -> x0, other arithmetic: 17.5 us -> none  [shards(): score_grad = weights * (prob_grad - delta)]
    pallas_call x0 -> x1, Pallas kernels: none -> 15.7 us  [attention(): pl.pallas_call(attention_kernel, grid=(heads,), in_specs=[pl.BlockSpec(me...]
    ppermute x4, waiting for transfers between devices: 10.7 us -> 24.2 us  [from_behind(): lax.ppermute(value, axis, [(source, source + steps) for source in range(l...]
    squeeze x4 -> x0, local copies, waits for them, and re-layouts: 9.99 us -> none  [fold_band(): shaped[:, band]]
  transfers between devices with their start and end apart: 7 -> 9, of which waited for: 4 -> 7; matrix products, arithmetic and copies ran while one was open for 26% -> 14% of each run, Pallas kernels for 0% -> 0%
where the time goes in v1:
time: 451 us; the launch traced here: 450 us
  waiting for transfers between devices  301 us (67%)
  matrix products  64.9 us (14%)
  blocking collectives  29.6 us (7%)
  Pallas kernels  15.7 us (3%)
  between operations  14 us (3%)
  local copies, waits for them, and re-layouts  13.4 us (3%)
  starting transfers between devices  10.1 us (2%)
    reduce_scatter x3, waiting for transfers between devices, reduce_weight(): lax.psum_scatter(part, 'sp', scatter_dimension=0, tiled=True)  170 us
    reduce_scatter x1, waiting for transfers between devices, shards(): lax.psum_scatter(input_part.astype(jnp.bfloat16), 'tp', scatter_dimension...  58.3 us
    all_gather x1, waiting for transfers between devices, shards(): whole = lax.all_gather(tokens, 'tp', axis=1, tiled=True)  48 us
    dot_general x3, matrix products, contract_cols(): lax.dot_general(left, right, (((1,), (1,)), ((), ())), preferred_element_...  29.7 us
    psum x1, blocking collectives, shards(): bias_grad = lax.psum(bias_local, 'sp')  29.6 us
    ppermute x4, waiting for transfers between devices, from_behind(): lax.ppermute(value, axis, [(source, source + steps) for source in range(l...  24.2 us
    dot_general x3, matrix products, contract_rows(): lax.dot_general(left, right, (((0,), (0,)), ((), ())), preferred_element_...  20.8 us
    pallas_call x1, Pallas kernels, attention(): pl.pallas_call(attention_kernel, grid=(heads,), in_specs=[pl.BlockSpec(me...  15.7 us
  transfers between devices with their start and end apart: 9, of which 7 were waited for; matrix products, arithmetic and copies ran while one was open for 14% of the time, Pallas kernels for 0%

profile of v1, /device:TPU:0, one launch (start us, length us, event | category | flops | bytes accessed | tf_op | source)
XLA Modules:
  0.0 450.3 jit_solution(4679994028842638057)
XLA Ops:
  7.2 0.0 all-gather.2.cloned.1.call-start
  7.2 0.7 all-gather.2.cloned.1.call-update
  7.9 0.0 reduce-scatter.7.cloned.1.call-start
  8.0 1.5 reverse
  9.5 0.1 slice.50
  9.6 0.1 pad.8.clone
  9.6 0.9 slice_reduce_fusion.1
  10.5 0.1 broadcast_in_dim.14
  10.6 0.1 maximum_maximum_fusion
  10.7 48.0 %all-gather.2.cloned.1.call-done = bf16[768,4096]{1,0:T(8,128)(2,1)} async-done(((bf16[768,1024]{1,0:T(8,128)(2,1)}), bf16[768,4096]{1,0:T(8,128)(2,1)}) %all-gather.2.cloned.1.call-update) | async-done | bytes 6291472 | tf_op jit(solution)/shard_map/all_gather | solution.py:154
  58.7 7.6 %convolution_convert_fusion.3.v_ref = bf16[768,512]{1,0:T(8,128)(2,1)S(1)} fusion(bf16[768,4096]{1,0:T(8,128)(2,1)} %all-gather.2.cloned.1.call-done, bf16[4096,512]{1,0:T(8,128)(2,1)} %param.9), kind=kOutput, calls=%fused_computation.7 | convolution fusion | flops 3221618688 | bytes 11272192 | tf_op jit(solution)/shard_map/dot_general | solution.py:159
  66.2 0.0 copy-start.2
  66.3 3.6 collective-permute-start.1
  69.9 0.0 copy-done.5
  69.9 0.0 copy-done.6
  69.9 3.4 convolution_convert_fusion.4.k_ref
  73.4 0.0 copy-start.1
  73.4 3.5 collective-permute-start
  76.9 0.0 copy-done.2
  76.9 3.4 convolution_convert_fusion.5.q_ref
  80.3 0.0 collective-permute-done.1.pv_ref
  80.3 2.2 collective-permute-done.pk_ref
  82.6 0.0 copy-done.1
  82.6 15.7 %segment_attention.1 = (bf16[768,512]{1,0:T(8,128)(2,1)S(1)}, f32[768,512]{1,0:T(8,128)S(1)}, f32[768,512]{1,0:T(8,128)S(1)}, bf16[256,512]{1,0:T(8,128)(2,1)S(1...) custom-call(s32[1]{0:T(128)} %bitcast.first_ref, bf16[768,512]{1,0:T(8,128)(2,1)S(1)} %convolution_convert_fusion.5.q_ref, ...), custom_call_target="tpu_custom_call" | custom-call | flops 1509949440 | bytes 4718592 | tf_op jit(solution)/shard_map/segment_attention/pallas_call | solution.py:111
  98.3 0.0 copy-start
  98.3 1.1 copy-done
  99.4 5.1 %fusion = bf16[4096,512]{0,1:T(8,128)(2,1)} fusion(bf16[768,512]{1,0:T(8,128)(2,1)S(1)} %get-tuple-element.11, bf16[768,4096]{1,0:T(8,128)(2,1)S(1)} %copy-done.5), kind=kOutput, calls=%fused_computation.4 | convolution fusion | flops 3223322624 | bytes 11272192 | tf_op jit(solution)/shard_map/dot_general | solution.py:24
  104.6 0.0 reduce-scatter.7.cloned.1.call-update
  104.6 0.0 reduce-scatter.11.cloned.1.call-start
  104.6 1.5 collective-permute-start.3
  106.1 1.3 slice.52
  107.4 7.2 %collective-permute-done.3 = bf16[256,512]{1,0:T(8,128)(2,1)S(1)} collective-permute-done((bf16[256,512]{1,0:T(8,128)(2,1)S(1)}, bf16[256,512]{1,0:T(8,128)(2,1)S(1)}, u32[]{:S(2)}, u32[]{:S(2)}) %collective-permute-start.3) | collective-permute-done | bytes 262176 | tf_op jit(solution)/shard_map/ppermute | solution.py:20
  114.6 1.1 add_convert_fusion.1
  115.7 7.8 %fusion.2 = bf16[4096,512]{0,1:T(8,128)(2,1)} fusion(bf16[768,4096]{1,0:T(8,128)(2,1)} %all-gather.2.cloned.1.call-done, bf16[256,512]{1,0:T(8,128)(2,1)S(1)} %add_convert_fusion.1, bf16[512,512]{1,0:T(8,128)(2,1)S(1)} %slice.52), kind=kOutput, calls=%fused_computation.6 | convolution fusion | flops 3224895488 | bytes 11272192 | tf_op jit(solution)/shard_map/dot_general | solution.py:24
  123.5 0.0 reduce-scatter.11.cloned.1.call-update
  123.6 0.0 reduce-scatter.9.cloned.1.call-start
  123.6 1.3 collective-permute-start.2
  124.9 0.1 slice.53
  125.0 0.0 copy-start.3
  125.0 14.8 %collective-permute-done.2 = bf16[256,512]{1,0:T(8,128)(2,1)S(1)} collective-permute-done((bf16[256,512]{1,0:T(8,128)(2,1)S(1)}, bf16[256,512]{1,0:T(8,128)(2,1)S(1)}, u32[]{:S(2)}, u32[]{:S(2)}) %collective-permute-start.2) | collective-permute-done | bytes 262176 | tf_op jit(solution)/shard_map/ppermute | solution.py:20
  139.8 0.1 add_convert_fusion.2
  139.9 0.0 copy-done.3
  139.9 7.8 %fusion.1 = bf16[4096,512]{0,1:T(8,128)(2,1)} fusion(bf16[768,4096]{1,0:T(8,128)(2,1)} %all-gather.2.cloned.1.call-done, bf16[256,512]{1,0:T(8,128)(2,1)S(1)} %add_convert_fusion.2, bf16[512,512]{1,0:T(8,128)(2,1)S(1)} %slice.53), kind=kOutput, calls=%fused_computation.5 | convolution fusion | flops 3224895488 | bytes 11272192 | tf_op jit(solution)/shard_map/dot_general | solution.py:24
  147.7 0.0 reduce-scatter.9.cloned.1.call-update
  147.7 0.0 reduce-scatter.5.cloned.1.call-start
  147.8 1.0 copy-done.4
  148.7 9.1 %fusion.4 = f32[768,4096]{1,0:T(8,128)} fusion(bf16[4096,512]{1,0:T(8,128)(2,1)} %param.8, bf16[256,512]{1,0:T(8,128)(2,1)S(1)} %add_convert_fusion.2, bf16[512,512]{1,0:T(8,128)(2,1)S(1)} %copy-done.4), kind=kOutput, calls=%fused_computation.17 | convolution fusion | flops 3222798336 | bytes 17563648 | tf_op jit(solution)/shard_map/dot_general | solution.py:30
  157.8 0.0 copy-done.7
  157.8 6.5 %fusion.3 = f32[768,4096]{1,0:T(8,128)} fusion(bf16[4096,512]{1,0:T(8,128)(2,1)S(1)} %copy-done.7, bf16[256,512]{1,0:T(8,128)(2,1)S(1)} %add_convert_fusion.1, bf16[512,512]{1,0:T(8,128)(2,1)S(1)} %slice.52), kind=kOutput, calls=%fused_computation.16 | convolution fusion | flops 3222798336 | bytes 17563648 | tf_op jit(solution)/shard_map/dot_general | solution.py:30
  164.3 14.1 %add_convert_fusion = bf16[768,4096]{1,0:T(8,128)(2,1)} fusion(f32[768,4096]{1,0:T(8,128)} %fusion.3, f32[768,4096]{1,0:T(8,128)} %fusion.4, bf16[768,512]{1,0:T(8,128)(2,1)S(1)} %get-tuple-element.11, bf16[4096,512]{1,0:T(8,128)(2,1)} %param.7), kind=kOutput, calls=%fused_computation | convolution fusion | flops 3230662656 | bytes 36438016 | tf_op jit(solution)/shard_map/dot_general | solution.py:30
  178.5 0.0 reduce-scatter.5.cloned.1.call-update
  178.5 0.1 slice.42
  178.6 0.3 reverse.1
  178.9 0.1 slice.51
  178.9 0.1 slice_reduce_fusion
  179.0 0.1 copy.11
  179.1 0.1 pad_maximum_fusion.6
  179.2 29.6 %psum.7 = f32[4,320]{1,0:T(4,128)} all-reduce(f32[4,320]{1,0:T(4,128)S(1)} %pad_maximum_fusion.6), channel_id=1, replica_groups=mesh['sp'=8,'tp'=4] {'sp'}, use_global_device_ids=true, to_apply=%region_5.0 | all-reduce | flops 1280 | bytes 10240 | tf_op jit(solution)/shard_map/psum | solution.py:193
  208.9 2.3 copy.12
  211.1 80.3 %reduce-scatter.11.cloned.1.call-done = bf16[512,512]{0,1:T(8,128)(2,1)} async-done(((bf16[4096,512]{0,1:T(8,128)(2,1)}), bf16[512,512]{0,1:T(8,128)(2,1)}) %reduce-scatter.11.cloned.1.call-update) | async-done | bytes 524304 | tf_op jit(solution)/shard_map/reduce_scatter | solution.py:178
  291.4 2.2 copy.14
  293.7 89.6 %reduce-scatter.9.cloned.1.call-done = bf16[512,512]{0,1:T(8,128)(2,1)} async-done(((bf16[4096,512]{0,1:T(8,128)(2,1)}), bf16[512,512]{0,1:T(8,128)(2,1)}) %reduce-scatter.9.cloned.1.call-update) | async-done | bytes 524304 | tf_op jit(solution)/shard_map/reduce_scatter | solution.py:178
  383.3 2.2 copy.13
  385.5 58.3 %reduce-scatter.5.cloned.1.call-done = bf16[768,1024]{1,0:T(8,128)(2,1)} async-done(((bf16[768,4096]{1,0:T(8,128)(2,1)}), bf16[768,1024]{1,0:T(8,128)(2,1)}) %reduce-scatter.5.cloned.1.call-update) | async-done | bytes 1572880 | tf_op jit(solution)/shard_map/reduce_scatter | solution.py:190
  (9 shorter events, 0.1 us)
Async XLA Ops:
  7.2 51.5 %all-gather.2.cloned.1.call-start = ((), (), s32[]{:S(2)}) async-start(), calls=%async_computation.4 | async-start | bytes 7864320 | tf_op jit(solution)/shard_map/all_gather | solution.py:154
  7.9 201.0 %reduce-scatter.7.cloned.1.call-start = ((), (), s32[]{:S(2)}) async-start(), calls=%async_computation.6 | async-start | bytes 4718592 | tf_op jit(solution)/shard_map/reduce_scatter | solution.py:178
  58.7 11.3 %copy-start.5 = (bf16[768,4096]{1,0:T(8,128)(2,1)S(1)}, bf16[768,4096]{1,0:T(8,128)(2,1)}, u32[]{:S(2)}) copy-start(bf16[768,4096]{1,0:T(8,128)(2,1)} %all-gather.2.cloned.1.call-done) | copy-start | bytes 18874372
  58.7 11.3 %copy-start.6 = (bf16[4096,512]{1,0:T(8,128)(2,1)S(1)}, bf16[4096,512]{1,0:T(8,128)(2,1)}, u32[]{:S(2)}) copy-start(bf16[4096,512]{1,0:T(8,128)(2,1)} %param.8) | copy-start | bytes 12582916
  66.2 10.7 %copy-start.2 = (bf16[4096,512]{1,0:T(8,128)(2,1)S(1)}, bf16[4096,512]{1,0:T(8,128)(2,1)}, u32[]{:S(2)}) copy-start(bf16[4096,512]{1,0:T(8,128)(2,1)} %param.7) | copy-start | bytes 12582916
  66.3 14.1 %collective-permute-start.1 = (bf16[256,512]{1,0:T(8,128)(2,1)S(1)}, bf16[256,512]{1,0:T(8,128)(2,1)S(1)}, u32[]{:S(2)}, u32[]{:S(2)}) collective-permute-start(bf16[256,512]{1,0:T(8,128)(2,1)S(1)} %slice.39), channel_id=1, source_target_pairs={{0,4},{4,8},{8,12},{12,16},{16,20},{20,24},{24,28},{1,5},{5,9},{9,... | collective-permute-start | bytes 786440 | tf_op jit(solution)/shard_map/ppermute | solution.py:20
  73.4 9.2 %copy-start.1 = (bf16[768,512]{1,0:T(8,128)(2,1)S(1)}, bf16[768,512]{1,0:T(8,128)(2,1)}, u32[]{:S(2)}) copy-start(bf16[768,512]{1,0:T(8,128)(2,1)} %g_ref.1) | copy-start | bytes 2359300
  73.4 9.2 %collective-permute-start = (bf16[256,512]{1,0:T(8,128)(2,1)S(1)}, bf16[256,512]{1,0:T(8,128)(2,1)S(1)}, u32[]{:S(2)}, u32[]{:S(2)}) collective-permute-start(bf16[256,512]{1,0:T(8,128)(2,1)S(1)} %slice.38), channel_id=1, source_target_pairs={{0,4},{4,8},{8,12},{12,16},{16,20},{20,24},{24,28},{1,5},{5,9},{9,... | collective-permute-start | bytes 786440 | tf_op jit(solution)/shard_map/ppermute | solution.py:20
  98.3 1.1 copy-start
  104.6 186.9 %reduce-scatter.11.cloned.1.call-start = ((), (), s32[]{:S(2)}) async-start(), calls=%async_computation.8 | async-start | bytes 4718592 | tf_op jit(solution)/shard_map/reduce_scatter | solution.py:178
  104.6 9.9 %collective-permute-start.3 = (bf16[256,512]{1,0:T(8,128)(2,1)S(1)}, bf16[256,512]{1,0:T(8,128)(2,1)S(1)}, u32[]{:S(2)}, u32[]{:S(2)}) collective-permute-start(bf16[256,512]{1,0:T(8,128)(2,1)S(1)} %get-tuple-element.15), channel_id=1, source_target_pairs={{4,0},{8,4},{12,8},{16,12},{20,16},{24,20},{28,24},{5,1},{9,5},{13... | collective-permute-start | bytes 786440 | tf_op jit(solution)/shard_map/ppermute | solution.py:20
  123.6 259.7 %reduce-scatter.9.cloned.1.call-start = ((), (), s32[]{:S(2)}) async-start(), calls=%async_computation.7 | async-start | bytes 4718592 | tf_op jit(solution)/shard_map/reduce_scatter | solution.py:178
  123.6 16.2 %collective-permute-start.2 = (bf16[256,512]{1,0:T(8,128)(2,1)S(1)}, bf16[256,512]{1,0:T(8,128)(2,1)S(1)}, u32[]{:S(2)}, u32[]{:S(2)}) collective-permute-start(bf16[256,512]{1,0:T(8,128)(2,1)S(1)} %get-tuple-element.13), channel_id=1, source_target_pairs={{4,0},{8,4},{12,8},{16,12},{20,16},{24,20},{28,24},{5,1},{9,5},{13... | collective-permute-start | bytes 786440 | tf_op jit(solution)/shard_map/ppermute | solution.py:20
  125.0 14.9 %copy-start.3 = (bf16[512,512]{1,0:T(8,128)(2,1)}, bf16[512,512]{1,0:T(8,128)(2,1)S(1)}, u32[]{:S(2)}) copy-start(bf16[512,512]{1,0:T(8,128)(2,1)S(1)} %slice.53) | copy-start | bytes 1572868
  147.7 1.0 copy-start.4
  147.7 296.1 %reduce-scatter.5.cloned.1.call-start = ((), (), s32[]{:S(2)}) async-start(), calls=%async_computation.5 | async-start | bytes 7864320 | tf_op jit(solution)/shard_map/reduce_scatter | solution.py:190
  148.7 9.1 %copy-start.7 = (bf16[4096,512]{1,0:T(8,128)(2,1)S(1)}, bf16[4096,512]{1,0:T(8,128)(2,1)}, u32[]{:S(2)}) copy-start(bf16[4096,512]{1,0:T(8,128)(2,1)} %param.9) | copy-start | bytes 12582916
Sparse Core Ops, SparseCore 0:
  9.5 49.0 all-gather.1
  104.7 94.5 reduce-scatter.6
  202.9 88.4 reduce-scatter.10
  294.9 88.3 reduce-scatter.8
  386.2 57.5 reduce-scatter.4

commit v2 on v1

--- a/solution.py
+++ b/solution.py
@@ -154,6 +154,19 @@
     whole = lax.all_gather(tokens, "tp", axis=1, tiled=True)
     length = whole.shape[0]
     cut = length - REACH
+    count = lax.axis_size("sp")
+    block = whole.shape[1] // count
+    side = lax.axis_index("sp") % 2
+    partners = [(index, index ^ 1) for index in range(count)]
+    groups = [list(range(start, count, 2)) for start in range(2)]
+
+    def rows_of(array, which):
+        cut_up = array.reshape(length, -1, 2, block)
+        return jnp.where(which == 0, cut_up[:, :, 0], cut_up[:, :, 1]).reshape(length, -1)
+
+    given = lax.ppermute(rows_of(tokens, 1 - side), "sp", partners)
+    other = lax.all_gather(given, "tp", axis=1, tiled=True)
+    paired = jnp.concatenate([rows_of(whole, side), other])
 
     def project(rows, weight):
         return jnp.dot(rows, weight, preferred_element_type=jnp.float32).astype(jnp.bfloat16)
@@ -174,8 +187,11 @@
         )
 
     def reduce_weight(grad):
-        part = contract_rows(whole, grad).astype(jnp.bfloat16)
-        return lax.psum_scatter(part, "sp", scatter_dimension=0, tiled=True).astype(jnp.float32)
+        pair = jnp.concatenate([grad, lax.ppermute(grad, "sp", partners)])
+        part = contract_rows(paired, pair).astype(jnp.bfloat16)
+        return lax.psum_scatter(
+            part, "sp", scatter_dimension=0, axis_index_groups=groups, tiled=True
+        ).astype(jnp.float32)
 
     query_weight_grad = reduce_weight(query_grad)
     key_grad = join(key_own, back_keys)

time: 451 us -> 335 us (0.74)
  waiting for transfers between devices: 301 us -> 163 us
  starting transfers between devices: 10.1 us -> 31.1 us
  other arithmetic: 1.46 us -> 14.3 us
  blocking collectives: 29.6 us -> 21.4 us
  local copies, waits for them, and re-layouts: 13.4 us -> 7.24 us
    reduce_scatter x3, waiting for transfers between devices: 170 us -> 9.69 us  [reduce_weight(): lax.psum_scatter(part, 'sp', scatter_dimension=0, axis_index_groups=group...]
    ppermute x0 -> x4, waiting for transfers between devices: none -> 53.8 us  [the longest x3 37.1 us: reduce_weight(): pair = jnp.concatenate([grad, lax.ppermute(grad, 'sp', partners)])]
    all_gather x1, waiting for transfers between devices: 48 us -> 26.4 us  [shards(): whole = lax.all_gather(tokens, 'tp', axis=1, tiled=True)]
    ppermute x0 -> x4, starting transfers between devices: none -> 20.1 us  [the longest x3 17.1 us: reduce_weight(): pair = jnp.concatenate([grad, lax.ppermute(grad, 'sp', partners)])]
    ppermute x4, waiting for transfers between devices: 24.2 us -> 15.3 us  [from_behind(): lax.ppermute(value, axis, [(source, source + steps) for source in range(l...]
    psum x1, blocking collectives: 29.6 us -> 21.4 us  [shards(): bias_grad = lax.psum(bias_local, 'sp')]
    convert_element_type x0 -> x3, other arithmetic: none -> 6.44 us  [reduce_weight(): return lax.psum_scatter(part, 'sp', scatter_dimension=0, axis_index_group...]
    select_n x0 -> x2, other arithmetic: none -> 6.28 us  [rows_of(): jnp.where(which == 0, cut_up[:, :, 0], cut_up[:, :, 1]).reshape(length, -1)]
  transfers between devices with their start and end apart: 9 -> 14, of which waited for: 7 -> 10; matrix products, arithmetic and copies ran while one was open for 14% -> 23% of each run, Pallas kernels for 0% -> 5%
where the time goes in v2:
time: 335 us; the launch traced here: 334 us
  waiting for transfers between devices  163 us (49%)
  matrix products  66.6 us (20%)
  starting transfers between devices  31.1 us (9%)
  blocking collectives  21.4 us (6%)
  Pallas kernels  15.7 us (5%)
  between operations  14.4 us (4%)
  other arithmetic  14.3 us (4%)
  local copies, waits for them, and re-layouts  7.24 us (2%)
    reduce_scatter x1, waiting for transfers between devices, shards(): lax.psum_scatter(input_part.astype(jnp.bfloat16), 'tp', scatter_dimension...  58.2 us
    ppermute x3, waiting for transfers between devices, reduce_weight(): pair = jnp.concatenate([grad, lax.ppermute(grad, 'sp', partners)])  37.1 us
    dot_general x3, matrix products, contract_cols(): lax.dot_general(left, right, (((1,), (1,)), ((), ())), preferred_element_...  31 us
    all_gather x1, waiting for transfers between devices, shards(): whole = lax.all_gather(tokens, 'tp', axis=1, tiled=True)  26.4 us
    psum x1, blocking collectives, shards(): bias_grad = lax.psum(bias_local, 'sp')  21.4 us
    dot_general x3, matrix products, contract_rows(): lax.dot_general(left, right, (((0,), (0,)), ((), ())), preferred_element_...  21.2 us
    ppermute x3, starting transfers between devices, reduce_weight(): pair = jnp.concatenate([grad, lax.ppermute(grad, 'sp', partners)])  17.1 us
    ppermute x1, waiting for transfers between devices, shards(): given = lax.ppermute(rows_of(tokens, 1 - side), 'sp', partners)  16.8 us
  transfers between devices with their start and end apart: 14, of which 10 were waited for; matrix products, arithmetic and copies ran while one was open for 23% of the time, Pallas kernels for 5%

profile of v2, /device:TPU:0, one launch (start us, length us, event | category | flops | bytes accessed | tf_op | source)
XLA Modules:
  0.0 334.1 jit_solution(3303226248696996055)
XLA Ops:
  7.2 0.0 all-gather.3.cloned.1.call-start
  7.2 2.6 copy.14
  9.8 0.0 all-gather.3.cloned.1.call-update
  9.8 0.0 all-gather.5.cloned.1.call-start
  9.9 1.5 fusion.13
  11.4 3.0 collective-permute-start.4
  14.4 0.3 reverse
  14.7 0.1 slice.76
  14.7 0.1 pad.18.clone
  14.8 0.2 slice_reduce_fusion.1
  15.0 0.1 broadcast_in_dim.14
  15.1 0.1 maximum_maximum_fusion
  15.2 16.8 %collective-permute-done.4 = bf16[768,512]{0,1:T(8,128)(2,1)S(1)} collective-permute-done((bf16[768,512]{0,1:T(8,128)(2,1)S(1)}, bf16[768,512]{0,1:T(8,128)(2,1)S(1)}, u32[]{:S(2)}, u32[]{:S(2)}) %collective-permute-start.4) | collective-permute-done | bytes 786464 | tf_op jit(solution)/shard_map/ppermute | solution.py:167
  31.9 0.9 copy-done.7
  32.8 0.0 all-gather.5.cloned.1.call-update
  32.8 0.0 reduce-scatter.7.cloned.1.call-start
  32.9 26.4 %all-gather.3.cloned.1.call-done = bf16[768,4096]{0,1:T(8,128)(2,1)} async-done(((bf16[768,1024]{0,1:T(8,128)(2,1)}), bf16[768,4096]{0,1:T(8,128)(2,1)}) %all-gather.3.cloned.1.call-update) | async-done | bytes 6291472 | tf_op jit(solution)/shard_map/all_gather | solution.py:154
  59.2 7.6 %convolution_convert_fusion.3.v_ref = bf16[768,512]{1,0:T(8,128)(2,1)S(1)} fusion(bf16[768,4096]{0,1:T(8,128)(2,1)} %all-gather.3.cloned.1.call-done, bf16[4096,512]{1,0:T(8,128)(2,1)} %param.9), kind=kOutput, calls=%fused_computation.19 | convolution fusion | flops 3221618688 | bytes 11272192 | tf_op jit(solution)/shard_map/dot_general | solution.py:172
  66.9 3.7 %collective-permute-start.1 = (bf16[256,512]{1,0:T(8,128)(2,1)S(1)}, bf16[256,512]{1,0:T(8,128)(2,1)S(1)}, u32[]{:S(2)}, u32[]{:S(2)}) collective-permute-start(bf16[256,512]{1,0:T(8,128)(2,1)S(1)} %slice.55), channel_id=1, source_target_pairs={{0,4},{4,8},{8,12},{12,16},{16,20},{20,24},{24,28},{1,5},{5,9},{9,... | collective-permute-start | bytes 786440 | tf_op jit(solution)/shard_map/ppermute | solution.py:20
  70.5 3.4 %convolution_convert_fusion.4.k_ref = bf16[768,512]{1,0:T(8,128)(2,1)S(1)} fusion(bf16[768,4096]{0,1:T(8,128)(2,1)S(1)} %copy-done.2, bf16[4096,512]{1,0:T(8,128)(2,1)S(1)} %copy-done.9), kind=kOutput, calls=%fused_computation.20 | convolution fusion | flops 3221618688 | bytes 11272192 | tf_op jit(solution)/shard_map/dot_general | solution.py:172
  74.0 3.7 %collective-permute-start = (bf16[256,512]{1,0:T(8,128)(2,1)S(1)}, bf16[256,512]{1,0:T(8,128)(2,1)S(1)}, u32[]{:S(2)}, u32[]{:S(2)}) collective-permute-start(bf16[256,512]{1,0:T(8,128)(2,1)S(1)} %slice.54), channel_id=1, source_target_pairs={{0,4},{4,8},{8,12},{12,16},{16,20},{20,24},{24,28},{1,5},{5,9},{9,... | collective-permute-start | bytes 786440 | tf_op jit(solution)/shard_map/ppermute | solution.py:20
  77.7 3.4 %convolution_convert_fusion.5.q_ref = bf16[768,512]{1,0:T(8,128)(2,1)S(1)} fusion(bf16[768,4096]{0,1:T(8,128)(2,1)S(1)} %copy-done.2, bf16[4096,512]{1,0:T(8,128)(2,1)S(1)} %copy-done.3), kind=kOutput, calls=%fused_computation.21 | convolution fusion | flops 3221618688 | bytes 11272192 | tf_op jit(solution)/shard_map/dot_general | solution.py:172
  81.2 2.0 collective-permute-done.pk_ref
  83.2 15.7 %segment_attention.1 = (bf16[768,512]{1,0:T(8,128)(2,1)S(1)}, f32[768,512]{1,0:T(8,128)S(1)}, f32[768,512]{1,0:T(8,128)S(1)}, bf16[256,512]{1,0:T(8,128)(2,1)S(1...) custom-call(s32[1]{0:T(128)} %bitcast.first_ref, bf16[768,512]{1,0:T(8,128)(2,1)S(1)} %convolution_convert_fusion.5.q_ref, ...), custom_call_target="tpu_custom_call" | custom-call | flops 1509949440 | bytes 4718592 | tf_op jit(solution)/shard_map/segment_attention/pallas_call | solution.py:111
  98.9 1.1 copy-done
  100.0 2.5 collective-permute-start.5
  102.5 4.8 %slice_select_fusion = bf16[768,4,1,512]{0,3,2,1:T(8,128)(2,1)} fusion(bf16[768,4,2,512]{0,3,2,1:T(8,128)(2,1)} %bitcast.24, pred[]{:T(512)S(6)} %eq.12), kind=kLoop, calls=%fused_computation.2 | loop fusion | flops 1572864 | bytes 9437185 | tf_op jit(solution)/shard_map/jit(_where)/select_n | solution.py:165
  107.4 12.2 %collective-permute-done.5 = bf16[768,512]{1,0:T(8,128)(2,1)} collective-permute-done((bf16[768,512]{1,0:T(8,128)(2,1)S(1)}, bf16[768,512]{1,0:T(8,128)(2,1)}, u32[]{:S(2)}, u32[]{:S(2)}) %collective-permute-start.5) | collective-permute-done | bytes 786464 | tf_op jit(solution)/shard_map/ppermute | solution.py:190
  119.6 7.7 %convolution_convert_fusion.2 = bf16[2048,512]{1,0:T(8,128)(2,1)} fusion(bf16[768,2048]{0,1:T(8,128)(2,1)} %all-gather.5.cloned.1.call-done, bf16[768,2048]{0,1:T(8,128)(2,1)} %bitcast.25, bf16[768,512]{1,0:T(8,128)(2,1)} %collective-permute-done.5, bf16[768,512]{1,0:T(8,128)(2,1)S(1)} %get-tuple-element.11), kind=kOutput, calls=%fused_computation.5 | convolution fusion | flops 3238002688 | bytes 9961472 | tf_op jit(solution)/shard_map/dot_general | solution.py:24
  127.3 0.0 reduce-scatter.9.cloned.1.call-start
  127.4 1.6 collective-permute-start.2
  128.9 1.3 slice.79
  130.2 6.1 %collective-permute-done.2 = bf16[256,512]{1,0:T(8,128)(2,1)S(1)} collective-permute-done((bf16[256,512]{1,0:T(8,128)(2,1)S(1)}, bf16[256,512]{1,0:T(8,128)(2,1)S(1)}, u32[]{:S(2)}, u32[]{:S(2)}) %collective-permute-start.2) | collective-permute-done | bytes 262176 | tf_op jit(solution)/shard_map/ppermute | solution.py:20
  136.4 1.1 add_convert_fusion.2
  137.5 0.1 pad_maximum_fusion.4
  137.5 7.6 %collective-permute-start.6 = (bf16[768,512]{1,0:T(8,128)(2,1)S(1)}, bf16[768,512]{1,0:T(8,128)(2,1)S(1)}, u32[]{:S(2)}, u32[]{:S(2)}) collective-permute-start(bf16[768,512]{1,0:T(8,128)(2,1)S(1)} %pad_maximum_fusion.4), channel_id=1, source_target_pairs={{0,4},{4,0},{8,12},{12,8},{16,20},{20,16},{24,28},{28,24},{1,5},{5... | collective-permute-start | bytes 2359304 | tf_op jit(solution)/shard_map/ppermute | solution.py:190
  145.1 10.2 %collective-permute-done.6 = bf16[768,512]{1,0:T(8,128)(2,1)S(1)} collective-permute-done((bf16[768,512]{1,0:T(8,128)(2,1)S(1)}, bf16[768,512]{1,0:T(8,128)(2,1)S(1)}, u32[]{:S(2)}, u32[]{:S(2)}) %collective-permute-start.6) | collective-permute-done | bytes 786464 | tf_op jit(solution)/shard_map/ppermute | solution.py:190
  155.3 6.7 %convolution_convert_fusion.1 = bf16[2048,512]{1,0:T(8,128)(2,1)} fusion(bf16[768,2048]{0,1:T(8,128)(2,1)} %all-gather.5.cloned.1.call-done, bf16[768,2048]{0,1:T(8,128)(2,1)S(1)} %bitcast.26, bf16[768,512]{1,0:T(8,128)(2,1)S(1)} %collective-permute-done.6, bf16[256,512]{1,0:T(8,128)(2,1)S(1)} %add_convert_fusion.2, bf16[512,512]{1,0:T(8,128)(2,1)S(1)} %slice.79), kind=kOutput, calls=%fused_computation.4 | convolution fusion | flops 3239575552 | bytes 9961472 | tf_op jit(solution)/shard_map/dot_general | solution.py:24
  162.0 0.0 reduce-scatter.9.cloned.1.call-update
  162.0 0.0 reduce-scatter.11.cloned.1.call-start
  162.1 1.8 collective-permute-start.3
  163.9 0.1 slice.78
  164.0 7.1 %collective-permute-done.3 = bf16[256,512]{1,0:T(8,128)(2,1)S(1)} collective-permute-done((bf16[256,512]{1,0:T(8,128)(2,1)S(1)}, bf16[256,512]{1,0:T(8,128)(2,1)S(1)}, u32[]{:S(2)}, u32[]{:S(2)}) %collective-permute-start.3) | collective-permute-done | bytes 262176 | tf_op jit(solution)/shard_map/ppermute | solution.py:20
  171.1 0.1 add_convert_fusion.1
  171.2 0.1 pad_maximum_fusion.5
  171.2 7.0 %collective-permute-start.7 = (bf16[768,512]{1,0:T(8,128)(2,1)S(1)}, bf16[768,512]{1,0:T(8,128)(2,1)S(1)}, u32[]{:S(2)}, u32[]{:S(2)}) collective-permute-start(bf16[768,512]{1,0:T(8,128)(2,1)S(1)} %pad_maximum_fusion.5), channel_id=1, source_target_pairs={{0,4},{4,0},{8,12},{12,8},{16,20},{20,16},{24,28},{28,24},{1,5},{5... | collective-permute-start | bytes 2359304 | tf_op jit(solution)/shard_map/ppermute | solution.py:190
  178.3 14.7 %collective-permute-done.7 = bf16[768,512]{1,0:T(8,128)(2,1)S(1)} collective-permute-done((bf16[768,512]{1,0:T(8,128)(2,1)S(1)}, bf16[768,512]{1,0:T(8,128)(2,1)S(1)}, u32[]{:S(2)}, u32[]{:S(2)}) %collective-permute-start.7) | collective-permute-done | bytes 786464 | tf_op jit(solution)/shard_map/ppermute | solution.py:190
  193.0 6.8 %convolution_convert_fusion = bf16[2048,512]{1,0:T(8,128)(2,1)} fusion(bf16[768,2048]{0,1:T(8,128)(2,1)} %all-gather.5.cloned.1.call-done, bf16[768,2048]{0,1:T(8,128)(2,1)S(1)} %bitcast.27, bf16[768,512]{1,0:T(8,128)(2,1)S(1)} %collective-permute-done.7, bf16[256,512]{1,0:T(8,128)(2,1)S(1)} %add_convert_fusion.1, bf16[512,512]{1,0:T(8,128)(2,1)S(1)} %slice.78), kind=kOutput, calls=%fused_computation.3 | convolution fusion | flops 3239575552 | bytes 9961472 | tf_op jit(solution)/shard_map/dot_general | solution.py:24
  199.7 0.0 reduce-scatter.5.cloned.1.call-start
  199.8 10.5 %fusion.17 = f32[768,4096]{1,0:T(8,128)} fusion(bf16[4096,512]{1,0:T(8,128)(2,1)} %param.9, bf16[256,512]{1,0:T(8,128)(2,1)S(1)} %add_convert_fusion.1, bf16[512,512]{1,0:T(8,128)(2,1)} %copy-done.6), kind=kOutput, calls=%fused_computation.38 | convolution fusion | flops 3222798336 | bytes 17563648 | tf_op jit(solution)/shard_map/dot_general | solution.py:30
  210.3 6.3 %fusion.18 = f32[768,4096]{1,0:T(8,128)} fusion(bf16[4096,512]{1,0:T(8,128)(2,1)S(1)} %copy-done.10, bf16[256,512]{1,0:T(8,128)(2,1)S(1)} %add_convert_fusion.2, bf16[512,512]{1,0:T(8,128)(2,1)S(1)} %slice.79), kind=kOutput, calls=%fused_computation.39 | convolution fusion | flops 3222798336 | bytes 17563648 | tf_op jit(solution)/shard_map/dot_general | solution.py:30
  216.6 14.2 %add_convert_fusion = bf16[768,4096]{1,0:T(8,128)(2,1)} fusion(f32[768,4096]{1,0:T(8,128)} %fusion.17, f32[768,4096]{1,0:T(8,128)} %fusion.18, bf16[768,512]{1,0:T(8,128)(2,1)S(1)} %get-tuple-element.11, bf16[4096,512]{1,0:T(8,128)(2,1)} %param.7), kind=kOutput, calls=%fused_computation | convolution fusion | flops 3230662656 | bytes 36438016 | tf_op jit(solution)/shard_map/dot_general | solution.py:30
  230.9 0.1 slice.62
  230.9 0.3 reverse.1
  231.2 0.1 slice.77
  231.3 0.1 slice_reduce_fusion
  231.4 0.1 copy.18
  231.5 0.1 pad_maximum_fusion.6
  231.6 21.4 %psum.7 = f32[4,320]{1,0:T(4,128)} all-reduce(f32[4,320]{1,0:T(4,128)S(1)} %pad_maximum_fusion.6), channel_id=1, replica_groups=mesh['sp'=8,'tp'=4] {'sp'}, use_global_device_ids=true, to_apply=%region_5.6 | all-reduce | flops 1280 | bytes 10240 | tf_op jit(solution)/shard_map/psum | solution.py:209
  253.0 2.1 convert_element_type.46
  255.1 2.1 convert_element_type.48
  257.3 9.7 %reduce-scatter.11.cloned.1.call-done = bf16[512,512]{1,0:T(8,128)(2,1)} async-done(((bf16[2048,512]{1,0:T(8,128)(2,1)}), bf16[512,512]{1,0:T(8,128)(2,1)}) %reduce-scatter.11.cloned.1.call-update) | async-done | bytes 524304 | tf_op jit(solution)/shard_map/reduce_scatter | solution.py:192
  266.9 2.1 convert_element_type.50
  269.1 58.2 %reduce-scatter.5.cloned.1.call-done = bf16[768,1024]{1,0:T(8,128)(2,1)} async-done(((bf16[768,4096]{1,0:T(8,128)(2,1)}), bf16[768,1024]{1,0:T(8,128)(2,1)}) %reduce-scatter.5.cloned.1.call-update) | async-done | bytes 1572880 | tf_op jit(solution)/shard_map/reduce_scatter | solution.py:206
  (31 shorter events, 0.2 us)
Async XLA Ops:
  7.2 7.2 %copy-start.8 = (f32[4,320]{1,0:T(4,128)S(1)}, f32[4,320]{1,0:T(4,128)}, u32[]{:S(2)}) copy-start(f32[4,320]{1,0:T(4,128)} %param.10) | copy-start | bytes 15364
  7.2 52.1 %all-gather.3.cloned.1.call-start = ((), (), s32[]{:S(2)}) async-start(), calls=%async_computation.4 | async-start | bytes 7864320 | tf_op jit(solution)/shard_map/all_gather | solution.py:154
  9.8 97.5 %all-gather.5.cloned.1.call-start = ((), (), s32[]{:S(2)}) async-start(), calls=%async_computation.6 | async-start | bytes 3932160 | tf_op jit(solution)/shard_map/all_gather | solution.py:168
  11.4 20.6 %collective-permute-start.4 = (bf16[768,512]{0,1:T(8,128)(2,1)S(1)}, bf16[768,512]{0,1:T(8,128)(2,1)S(1)}, u32[]{:S(2)}, u32[]{:S(2)}) collective-permute-start(bf16[768,512]{0,1:T(8,128)(2,1)S(1)} %fusion.13), channel_id=1, source_target_pairs={{0,4},{4,0},{8,12},{12,8},{16,20},{20,16},{24,28},{28,24},{1,5},{5... | collective-permute-start | bytes 2359304 | tf_op jit(solution)/shard_map/ppermute | solution.py:167
  31.9 0.9 copy-start.7
  32.8 220.1 %reduce-scatter.7.cloned.1.call-start = ((), (), s32[]{:S(2)}) async-start(), calls=%async_computation.7 | async-start | bytes 2621440 | tf_op jit(solution)/shard_map/reduce_scatter | solution.py:192
  59.2 11.3 %copy-start.2 = (bf16[768,4096]{0,1:T(8,128)(2,1)S(1)}, bf16[768,4096]{0,1:T(8,128)(2,1)}, u32[]{:S(2)}) copy-start(bf16[768,4096]{0,1:T(8,128)(2,1)} %all-gather.3.cloned.1.call-done) | copy-start | bytes 18874372
  59.2 11.3 %copy-start.9 = (bf16[4096,512]{1,0:T(8,128)(2,1)S(1)}, bf16[4096,512]{1,0:T(8,128)(2,1)}, u32[]{:S(2)}) copy-start(bf16[4096,512]{1,0:T(8,128)(2,1)} %param.8) | copy-start | bytes 12582916
  66.8 10.9 %copy-start.3 = (bf16[4096,512]{1,0:T(8,128)(2,1)S(1)}, bf16[4096,512]{1,0:T(8,128)(2,1)}, u32[]{:S(2)}) copy-start(bf16[4096,512]{1,0:T(8,128)(2,1)} %param.7) | copy-start | bytes 12582916
  66.9 14.3 %collective-permute-start.1 = (bf16[256,512]{1,0:T(8,128)(2,1)S(1)}, bf16[256,512]{1,0:T(8,128)(2,1)S(1)}, u32[]{:S(2)}, u32[]{:S(2)}) collective-permute-start(bf16[256,512]{1,0:T(8,128)(2,1)S(1)} %slice.55), channel_id=1, source_target_pairs={{0,4},{4,8},{8,12},{12,16},{16,20},{20,24},{24,28},{1,5},{5,9},{9,... | collective-permute-start | bytes 786440 | tf_op jit(solution)/shard_map/ppermute | solution.py:20
  74.0 9.2 %copy-start.1 = (bf16[768,512]{1,0:T(8,128)(2,1)S(1)}, bf16[768,512]{1,0:T(8,128)(2,1)}, u32[]{:S(2)}) copy-start(bf16[768,512]{1,0:T(8,128)(2,1)} %g_ref.1) | copy-start | bytes 2359300
  74.0 9.2 %collective-permute-start = (bf16[256,512]{1,0:T(8,128)(2,1)S(1)}, bf16[256,512]{1,0:T(8,128)(2,1)S(1)}, u32[]{:S(2)}, u32[]{:S(2)}) collective-permute-start(bf16[256,512]{1,0:T(8,128)(2,1)S(1)} %slice.54), channel_id=1, source_target_pairs={{0,4},{4,8},{8,12},{12,16},{16,20},{20,24},{24,28},{1,5},{5,9},{9,... | collective-permute-start | bytes 786440 | tf_op jit(solution)/shard_map/ppermute | solution.py:20
  98.9 1.1 copy-start
  100.0 19.5 %collective-permute-start.5 = (bf16[768,512]{1,0:T(8,128)(2,1)S(1)}, bf16[768,512]{1,0:T(8,128)(2,1)}, u32[]{:S(2)}, u32[]{:S(2)}) collective-permute-start(bf16[768,512]{1,0:T(8,128)(2,1)S(1)} %get-tuple-element.11), channel_id=1, source_target_pairs={{0,4},{4,0},{8,12},{12,8},{16,20},{20,16},{24,28},{28,24},{1,5},{5... | collective-permute-start | bytes 2359304 | tf_op jit(solution)/shard_map/ppermute | solution.py:190
  127.3 127.8 %reduce-scatter.9.cloned.1.call-start = ((), (), s32[]{:S(2)}) async-start(), calls=%async_computation.8 | async-start | bytes 2621440 | tf_op jit(solution)/shard_map/reduce_scatter | solution.py:192
  127.4 28.0 %copy-start.4 = (bf16[768,4,1,512]{0,3,2,1:T(8,128)(2,1)S(1)}, bf16[768,4,1,512]{0,3,2,1:T(8,128)(2,1)}, u32[]{:S(2)}) copy-start(bf16[768,4,1,512]{0,3,2,1:T(8,128)(2,1)} %slice_select_fusion) | copy-start | bytes 9437188
  127.4 9.0 %collective-permute-start.2 = (bf16[256,512]{1,0:T(8,128)(2,1)S(1)}, bf16[256,512]{1,0:T(8,128)(2,1)S(1)}, u32[]{:S(2)}, u32[]{:S(2)}) collective-permute-start(bf16[256,512]{1,0:T(8,128)(2,1)S(1)} %get-tuple-element.13), channel_id=1, source_target_pairs={{4,0},{8,4},{12,8},{16,12},{20,16},{24,20},{28,24},{5,1},{9,5},{13... | collective-permute-start | bytes 786440 | tf_op jit(solution)/shard_map/ppermute | solution.py:20
  137.5 17.8 %collective-permute-start.6 = (bf16[768,512]{1,0:T(8,128)(2,1)S(1)}, bf16[768,512]{1,0:T(8,128)(2,1)S(1)}, u32[]{:S(2)}, u32[]{:S(2)}) collective-permute-start(bf16[768,512]{1,0:T(8,128)(2,1)S(1)} %pad_maximum_fusion.4), channel_id=1, source_target_pairs={{0,4},{4,0},{8,12},{12,8},{16,20},{20,16},{24,28},{28,24},{1,5},{5... | collective-permute-start | bytes 2359304 | tf_op jit(solution)/shard_map/ppermute | solution.py:190
  162.0 104.9 %reduce-scatter.11.cloned.1.call-start = ((), (), s32[]{:S(2)}) async-start(), calls=%async_computation.9 | async-start | bytes 2621440 | tf_op jit(solution)/shard_map/reduce_scatter | solution.py:192
  162.1 30.9 %copy-start.5 = (bf16[768,4,1,512]{0,3,2,1:T(8,128)(2,1)S(1)}, bf16[768,4,1,512]{0,3,2,1:T(8,128)(2,1)}, u32[]{:S(2)}) copy-start(bf16[768,4,1,512]{0,3,2,1:T(8,128)(2,1)} %slice_select_fusion) | copy-start | bytes 9437188
  162.1 9.0 %collective-permute-start.3 = (bf16[256,512]{1,0:T(8,128)(2,1)S(1)}, bf16[256,512]{1,0:T(8,128)(2,1)S(1)}, u32[]{:S(2)}, u32[]{:S(2)}) collective-permute-start(bf16[256,512]{1,0:T(8,128)(2,1)S(1)} %get-tuple-element.15), channel_id=1, source_target_pairs={{4,0},{8,4},{12,8},{16,12},{20,16},{24,20},{28,24},{5,1},{9,5},{13... | collective-permute-start | bytes 786440 | tf_op jit(solution)/shard_map/ppermute | solution.py:20
  163.9 29.0 %copy-start.6 = (bf16[512,512]{1,0:T(8,128)(2,1)}, bf16[512,512]{1,0:T(8,128)(2,1)S(1)}, u32[]{:S(2)}) copy-start(bf16[512,512]{1,0:T(8,128)(2,1)S(1)} %slice.78) | copy-start | bytes 1572868
  171.2 21.7 %collective-permute-start.7 = (bf16[768,512]{1,0:T(8,128)(2,1)S(1)}, bf16[768,512]{1,0:T(8,128)(2,1)S(1)}, u32[]{:S(2)}, u32[]{:S(2)}) collective-permute-start(bf16[768,512]{1,0:T(8,128)(2,1)S(1)} %pad_maximum_fusion.5), channel_id=1, source_target_pairs={{0,4},{4,0},{8,12},{12,8},{16,20},{20,16},{24,28},{28,24},{1,5},{5... | collective-permute-start | bytes 2359304 | tf_op jit(solution)/shard_map/ppermute | solution.py:190
  199.7 127.5 %reduce-scatter.5.cloned.1.call-start = ((), (), s32[]{:S(2)}) async-start(), calls=%async_computation.5 | async-start | bytes 7864320 | tf_op jit(solution)/shard_map/reduce_scatter | solution.py:206
  199.8 10.5 %copy-start.10 = (bf16[4096,512]{1,0:T(8,128)(2,1)S(1)}, bf16[4096,512]{1,0:T(8,128)(2,1)}, u32[]{:S(2)}) copy-start(bf16[4096,512]{1,0:T(8,128)(2,1)} %param.8) | copy-start | bytes 12582916
Sparse Core Ops, SparseCore 0:
  10.1 49.0 all-gather.2
  61.4 28.5 all-gather.4
  127.4 49.6 reduce-scatter.6
  179.3 42.0 reduce-scatter.8
  223.6 43.3 reduce-scatter.10
  269.9 57.2 reduce-scatter.4
